TPU v7x, 256 devices: a whole 4x4x8 slice. The times are simulated.
256 devices in a mesh: sp: 16 (over y, x), tp: 16 (over z, core).
Axes of the slice: x: 4, y: 4, z: 8, core: 2. Of those that a mesh axis runs over, the one named last changes fastest.
Arguments:
- conv_value: bfloat16 [49152, 2048], P('sp', 'tp'), may hold values from -48 to 48
- conv_gate: bfloat16 [49152, 2048], P('sp', 'tp'), may hold values from -6 to 6
- doc_ids: int32 [49152], P('sp'), may hold values from 0 to 15, never falling along the last dimension, each value on 1 to 9216 neighbouring positions
- conv_kernel: bfloat16 [31, 2048], P(None, 'tp'), may hold values from -1 to 1
- norm_gain_conv: float32 [2048], replicated, may hold values from 0.1 to 1.9
- norm_bias_conv: float32 [2048], replicated, may hold values from -3 to 3
- proj_weight: bfloat16 [2048, 2048], P('tp'), may hold values from -0.125 to 0.125
- residual: bfloat16 [49152, 2048], P(('sp', 'tp')), may hold values from -6 to 6
- norm_gain_moe: float32 [2048], replicated, may hold values from 0.1 to 1.9
- group_router: bfloat16 [2048, 2], replicated, may hold values from -0.125 to 0.125
- expert_router: bfloat16 [2048, 16], replicated, may hold values from -0.125 to 0.125
- routing: int32 [49152, 2], P(('sp', 'tp')), may hold values from 0 to 15, as said below
- expert_gate_w: bfloat16 [16, 2048, 512], P('sp'), may hold values from -0.125 to 0.125
- expert_up_w: bfloat16 [16, 2048, 512], P('sp'), may hold values from -0.125 to 0.125
- expert_down_w: bfloat16 [16, 512, 2048], P('sp'), may hold values from -0.25 to 0.25
Outputs:
- output: bfloat16 [49152, 2048], P(('sp', 'tp'))
Inputs may be any that keep to these rules, and one draw needn't show every extreme that they name: `routing`: both numbers of a row are different experts of one group (expert // 8); within the rows of one device (aligned blocks of 192 rows) every expert is named exactly 24 times.
All inputs are finite; a program needn't handle non-finite values.
Results may differ from a plain program's by a relative error of at most 0.015.
Values may be sent and summed in bfloat16 or wider, within the bound.
No kernel may reach another device: no remote copies, remote signals or barrier semaphores. Data moves between devices by JAX's collectives and lax.ppermute only.
A program may use at most 64 MiB of HBM per device.

v0:
```python
import jax
import jax.numpy as jnp
from jax import lax
from jax.sharding import PartitionSpec as P

epsilon = 1e-06


def shifted(array, axis, by):
    count = lax.axis_size(axis)
    pairs = [(i, i + by) for i in range(count) if 0 <= i + by < count]
    return lax.ppermute(array, axis, pairs)


def project_rows(activated_rows, proj_weight):
    return jnp.dot(
        activated_rows,
        lax.all_gather(proj_weight, "tp", axis=0, tiled=True),
        preferred_element_type=jnp.float32,
    )


def body(
    conv_value,
    conv_gate,
    doc_ids,
    conv_kernel,
    norm_gain_conv,
    norm_bias_conv,
    proj_weight,
    residual,
    norm_gain_moe,
    group_router,
    expert_router,
    routing,
    expert_gate_w,
    expert_up_w,
    expert_down_w,
):
    local_tokens, local_width = conv_value.shape
    kernel_taps = conv_kernel.shape[0]
    rim_width = kernel_taps - 1
    gated_values = (
        conv_value.astype(jnp.float32) * jax.nn.sigmoid(conv_gate.astype(jnp.float32))
    ).astype(jnp.bfloat16)
    rim_values, rim_ids = shifted(
        (gated_values[local_tokens - rim_width :], doc_ids[local_tokens - rim_width :]), "sp", 1
    )
    padded = jnp.concatenate([rim_values, gated_values], axis=0)
    padded_ids = jnp.concatenate([rim_ids, doc_ids], axis=0)
    kernel = conv_kernel.astype(jnp.float32)
    summed = jnp.zeros((local_tokens, local_width), jnp.float32)
    for tap in range(kernel_taps):
        same_doc = padded_ids[tap : tap + local_tokens] == doc_ids
        summed = summed + jnp.where(
            same_doc[:, None],
            padded[tap : tap + local_tokens].astype(jnp.float32) * kernel[tap][None, :],
            jnp.float32(0.0),
        )
    convolved = summed.astype(jnp.bfloat16)
    raw_rows = lax.all_to_all(convolved, "tp", split_axis=0, concat_axis=1, tiled=True)
    raw_values = raw_rows.astype(jnp.float32)
    average = jnp.mean(raw_values, axis=1, keepdims=True)
    centered = raw_values - average
    variance = jnp.mean(centered * centered, axis=1, keepdims=True)
    moved_rows = jax.nn.silu(
        centered * lax.rsqrt(variance + epsilon) * norm_gain_conv + norm_bias_conv
    ).astype(jnp.bfloat16)
    projected = project_rows(moved_rows, proj_weight)
    state_values = residual.astype(jnp.float32) + projected
    hidden_state = state_values.astype(jnp.bfloat16)
    state_values = hidden_state.astype(jnp.float32)
    normed = (
        state_values
        * lax.rsqrt(jnp.mean(state_values * state_values, axis=1, keepdims=True) + epsilon)
        * norm_gain_moe
    ).astype(jnp.bfloat16)
    group_logits = jnp.dot(normed, group_router, preferred_element_type=jnp.float32)
    expert_logits = jnp.dot(normed, expert_router, preferred_element_type=jnp.float32)
    group_total = group_router.shape[1]
    expert_total = expert_router.shape[1]
    per_group = expert_total // group_total
    first_choice = routing[:, 0]
    second_choice = routing[:, 1]
    chosen_group = first_choice // per_group
    group_exp = jnp.exp(group_logits)
    group_match = chosen_group[:, None] == jnp.arange(group_total, dtype=jnp.int32)[None, :]
    group_prob = jnp.sum(jnp.where(group_match, group_exp, jnp.float32(0.0)), axis=1) / jnp.sum(
        group_exp, axis=1
    )
    expert_iota = jnp.arange(expert_total, dtype=jnp.int32)[None, :]
    first_logit = jnp.sum(
        jnp.where(first_choice[:, None] == expert_iota, expert_logits, jnp.float32(0.0)), axis=1
    )
    second_logit = jnp.sum(
        jnp.where(second_choice[:, None] == expert_iota, expert_logits, jnp.float32(0.0)), axis=1
    )
    first_exp = jnp.exp(first_logit)
    second_exp = jnp.exp(second_logit)
    first_weight = group_prob * first_exp / (first_exp + second_exp)
    second_weight = group_prob * second_exp / (first_exp + second_exp)
    row_count = normed.shape[0]
    capacity = 2 * row_count // expert_total
    flat_experts = routing.reshape(-1)
    indicator = (flat_experts[:, None] == expert_iota).astype(jnp.int32)
    before = jnp.cumsum(indicator, axis=0) - indicator
    position = jnp.sum(before * indicator, axis=1)
    destination = flat_experts * capacity + position
    source = (
        jnp.zeros((2 * row_count,), jnp.int32)
        .at[destination]
        .set(jnp.arange(2 * row_count, dtype=jnp.int32) // 2)
    )
    outgoing = normed[source].reshape(expert_total, capacity, normed.shape[1])
    arrived = lax.all_to_all(outgoing, "sp", split_axis=0, concat_axis=0, tiled=True)
    senders, slot_count, features = arrived.shape
    flattened = arrived.reshape(senders * slot_count, features)
    gate_part = jnp.dot(flattened, expert_gate_w[0], preferred_element_type=jnp.float32)
    up_part = jnp.dot(flattened, expert_up_w[0], preferred_element_type=jnp.float32)
    expert_hidden = (jax.nn.silu(gate_part) * up_part).astype(jnp.bfloat16)
    expert_result = jnp.dot(
        expert_hidden, expert_down_w[0], preferred_element_type=jnp.float32
    ).astype(jnp.bfloat16)
    returned = lax.all_to_all(
        expert_result.reshape(senders, slot_count, features),
        "sp",
        split_axis=0,
        concat_axis=0,
        tiled=True,
    )
    picked = (
        returned.reshape(2 * row_count, normed.shape[1])[destination]
        .reshape(row_count, 2, normed.shape[1])
        .astype(jnp.float32)
    )
    mixture = first_weight[:, None] * picked[:, 0] + second_weight[:, None] * picked[:, 1]
    return (state_values + mixture).astype(jnp.bfloat16)


def solution(mesh):
    placed = (
        P("sp", "tp"),
        P("sp", "tp"),
        P("sp"),
        P(None, "tp"),
        P(),
        P(),
        P("tp", None),
        P(("sp", "tp"), None),
        P(),
        P(),
        P(),
        P(("sp", "tp"), None),
        P("sp", None, None),
        P("sp", None, None),
        P("sp", None, None),
    )
    return jax.shard_map(
        body, mesh=mesh, in_specs=placed, out_specs=P(("sp", "tp"), None), check_vma=False
    )
```

profile of v0, /device:TPU:0, one launch (start us, length us, event | category | flops | bytes accessed | tf_op | source)
XLA Modules:
  0.0 186.5 jit_solution(3365401490658242660)
XLA Ops:
  6.5 0.0 copy-start
  6.5 0.0 all-gather.2.cloned.1.call-start
  6.5 0.7 all-gather.2.cloned.1.call-update
  7.3 0.8 slice.297
  8.0 1.7 collective-permute-start
  9.7 1.8 multiply_convert_fusion.2
  11.5 3.4 %collective-permute-start.1 = (bf16[30,128]{1,0:T(8,128)(2,1)S(1)}, bf16[30,128]{1,0:T(8,128)(2,1)S(1)}, u32[]{:S(2)}, u32[]{:S(2)}) collective-permute-start(bf16[30,128]{1,0:T(8,128)(2,1)S(1)} %slice.402), channel_id=1, source_target_pairs={{0,16},{16,32},{32,48},{48,64},{64,80},{80,96},{96,112},{112,128},... | collective-permute-start | bytes 23048 | tf_op jit(solution)/shard_map/ppermute | solution.py:12
  14.9 0.0 copy-done.9
  15.0 0.0 collective-permute-done
  15.0 0.0 copy-done.4
  15.0 0.1 fusion.72
  15.1 0.1 fusion.74
  15.2 0.1 fusion.76
  15.3 0.1 fusion.126
  15.4 0.8 collective-permute-done.1
  16.3 16.6 %add_convert_fusion = bf16[3072,128]{1,0:T(8,128)(2,1)} fusion(bf16[3072,128]{1,0:T(8,128)(2,1)S(1)} %multiply_convert_fusion.2, bf16[30,128]{1,0:T(8,128)(2,1)S(1)} %collective-permute-done.1, f32[128]{0:T(128)S(1)} %get-tuple-element.14, f32[128]{0:T(128)S(1)} %get-tuple-element.15, f32[128]{0:T(128)S(1)} %get-tuple-element.16, ...), kind=kLoop, calls=%fused_computation.60 | loop fusion | flops 83755008 | bytes 1688576 | tf_op jit(solution)/shard_map/convert_element_type | solution.py:60
  32.9 8.7 %all-to-all-start = ((bf16[16,192,128]{2,1,0:T(8,128)(2,1)}), bf16[16,192,128]{2,1,0:T(8,128)(2,1)S(1)}, u32[]{:S(2)}, u32[]{:S(2)}) async-start(bf16[16,192,128]{2,1,0:T(8,128)(2,1)} %bitcast.147), calls=%async_computation | async-start | bytes 1572864 | tf_op jit(solution)/shard_map/all_to_all | solution.py:61
  41.6 0.1 copy.25
  41.7 0.1 eq.206
  41.8 0.1 eq.202
  42.0 0.9 reduce-window.6
  42.9 0.2 slice_reduce_fusion
  43.1 0.1 copy.24
  43.3 0.1 mul.522
  43.4 0.1 fusion.67
  43.5 2.9 %scatter_custom_fusion = s32[384]{0:T(512)S(1)} fusion(s32[384]{0:T(512)S(1)} %fusion.132, s32[384]{0:T(512)S(1)} %add_select_fusion, s32[]{:T(128)} %constant.50.clone.1), kind=kCustom, calls=%fused_computation.261 | custom fusion | bytes 1540 | tf_op jit(solution)/shard_map/scatter | solution.py:112
  46.5 25.0 %all-to-all-done = bf16[16,192,128]{2,1,0:T(8,128)(2,1)S(1)} async-done(((bf16[16,192,128]{2,1,0:T(8,128)(2,1)}), bf16[16,192,128]{2,1,0:T(8,128)(2,1)S(1)}, u32[]{:S(2)}, u32[]{:S(2)}) %all-to-all-start) | async-done | bytes 786464 | tf_op jit(solution)/shard_map/all_to_all | solution.py:61
  71.5 0.2 convert_reduce_fusion
  71.7 0.4 fusion.8
  72.1 0.0 copy-start.7
  72.1 11.1 %all-gather.2.cloned.1.call-done = bf16[2048,2048]{1,0:T(8,128)(2,1)} async-done(((bf16[128,2048]{1,0:T(8,128)(2,1)}), bf16[2048,2048]{1,0:T(8,128)(2,1)}) %all-gather.2.cloned.1.call-update) | async-done | bytes 8388624 | tf_op jit(solution)/shard_map/all_gather | solution.py:18
  83.2 5.7 %multiply_reduce_fusion = (f32[192]{0:T(256)S(1)}, f32[192,2048]{1,0:T(8,128)S(1)}) fusion(bf16[2048,2048]{1,0:T(8,128)(2,1)} %all-gather.2.cloned.1.call-done, f32[2048]{0:T(1024)S(1)} %copy-done.11, f32[2048]{0:T(1024)S(1)} %copy-done.12, f32[192]{0:T(256)S(1)} %add_rsqrt_fusion.1, f32[192]{0:T(256)S(1)} %broadcast_multiply_fusion.1, ...), kind=kOutput, calls=%fused_computation.58 | convolution fusion | flops 1616903936 | bytes 11553024 | tf_op jit(solution)/shard_map/dot_general | solution.py:16
  88.9 1.1 copy-done.1
  90.0 0.2 multiply_convert_fusion
  90.2 3.1 %gather_fusion = bf16[384,2048]{1,0:T(8,128)(2,1)} fusion(bf16[192,2048]{1,0:T(8,128)(2,1)S(1)} %multiply_convert_fusion, s32[1024]{0:T(1024)S(1)} %pad_clamp_fusion.1), kind=kCustom, calls=%fused_computation | custom fusion | bytes 3147264 | tf_op jit(solution)/shard_map/gather | solution.py:114
  93.3 30.1 %all_to_all.23 = bf16[16,24,2048]{2,1,0:T(8,128)(2,1)S(1)} all-to-all(bf16[16,24,2048]{2,1,0:T(8,128)(2,1)} %bitcast.146), channel_id=1, replica_groups=mesh['sp'=16,'tp'=16] {'sp'}, dimensions={0} | all-to-all | bytes 3145728 | tf_op jit(solution)/shard_map/all_to_all | solution.py:115
  123.5 1.2 copy-done.3
  124.6 1.9 fusion.5
  126.5 5.3 %convolution_convert_fusion = bf16[384,2048]{1,0:T(8,128)(2,1)} fusion(bf16[1,512,2048]{2,1,0:T(8,128)(2,1)S(1)} %copy-done, bf16[384,2048]{1,0:T(8,128)(2,1)} %bitcast.150, bf16[1,2048,512]{2,1,0:T(8,128)(2,1)} %param.28, f32[384,512]{1,0:T(8,128)} %fusion.5), kind=kOutput, calls=%fused_computation.32 | convolution fusion | flops 1612578816 | bytes 8126464 | tf_op jit(solution)/shard_map/dot_general | solution.py:121
  131.8 4.7 %all-to-all-start.2 = ((bf16[16,24,2048]{2,1,0:T(8,128)(2,1)}), bf16[16,24,2048]{2,1,0:T(8,128)(2,1)}, u32[]{:S(2)}, u32[]{:S(2)}) async-start(bf16[16,24,2048]{2,1,0:T(8,128)(2,1)} %bitcast.148), calls=%async_computation.2 | async-start | bytes 3145728 | tf_op jit(solution)/shard_map/all_to_all | solution.py:124
  136.5 0.3 fusion.137
  136.9 0.3 select_reduce_fusion.1
  137.3 22.2 %all-to-all-done.2 = bf16[16,24,2048]{2,1,0:T(8,128)(2,1)} async-done(((bf16[16,24,2048]{2,1,0:T(8,128)(2,1)}), bf16[16,24,2048]{2,1,0:T(8,128)(2,1)}, u32[]{:S(2)}, u32[]{:S(2)}) %all-to-all-start.2) | async-done | bytes 1572896 | tf_op jit(solution)/shard_map/all_to_all | solution.py:124
  159.5 6.7 %gather_fusion.1 = bf16[384,2048]{1,0:T(8,128)(2,1)} fusion(bf16[384,2048]{1,0:T(8,128)(2,1)} %bitcast.43, s32[1024]{0:T(1024)S(1)} %pad_clamp_fusion), kind=kCustom, calls=%fused_computation.1 | custom fusion | bytes 3147264 | tf_op jit(solution)/shard_map/gather | solution.py:132
  166.2 4.7 %reshape.154 = f32[192,2,2048]{2,1,0:T(2,128)} reshape(bf16[384,2048]{1,0:T(8,128)(2,1)} %gather_fusion.1) | data formatting | bytes 4718592 | tf_op jit(solution)/shard_map/convert_element_type | solution.py:134
  170.9 6.2 %fusion.138 = (f32[192,1,2048]{2,1,0:T(1,128)S(1)}, f32[192,1,2048]{2,1,0:T(1,128)S(1)}) fusion(f32[192,2,2048]{2,1,0:T(2,128)} %reshape.154), kind=kLoop, calls=%fused_computation.302 | loop fusion | bytes 6291456 | tf_op jit(solution)/shard_map/slice | solution.py:136
  177.1 0.0 copy-done.2
  177.1 2.6 %fusion.15 = bf16[192,2048]{1,0:T(8,128)(2,1)} fusion(f32[192,2048]{1,0:T(8,128)S(1)} %copy-done.2, f32[192,1,2048]{2,1,0:T(1,128)S(1)} %get-tuple-element.12, f32[192,1,2048]{2,1,0:T(1,128)S(1)} %get-tuple-element.11, f32[192]{0:T(256)S(1)} %multiply_divide_fusion, f32[192]{0:T(256)S(1)} %get-tuple-element.9), kind=kLoop, calls=%fused_computation.54 | loop fusion | flops 1966080 | bytes 5506560 | tf_op jit(solution)/shard_map/convert_element_type | solution.py:137
  (37 shorter events, 0.2 us)
Async XLA Ops:
  6.5 119.9 %copy-start = (bf16[1,512,2048]{2,1,0:T(8,128)(2,1)S(1)}, bf16[1,512,2048]{2,1,0:T(8,128)(2,1)}, u32[]{:S(2)}) copy-start(bf16[1,512,2048]{2,1,0:T(8,128)(2,1)} %param.29) | copy-start | bytes 6291460
  6.5 8.5 %copy-start.4 = (s32[3072]{0:T(1024)S(1)}, s32[3072]{0:T(1024)}, u32[]{:S(2)}) copy-start(s32[3072]{0:T(1024)} %param.17) | copy-start | bytes 36868
  6.5 8.4 %copy-start.9 = (bf16[31,128]{1,0:T(8,128)(2,1)S(1)}, bf16[31,128]{1,0:T(8,128)(2,1)}, u32[]{:S(2)}) copy-start(bf16[31,128]{1,0:T(8,128)(2,1)} %param.18) | copy-start | bytes 23812
  6.5 76.6 %all-gather.2.cloned.1.call-start = ((), (), s32[]{:S(2)}) async-start(), calls=%async_computation.3 | async-start | bytes 8912896 | tf_op jit(solution)/shard_map/all_gather | solution.py:18
  8.0 7.0 %collective-permute-start = (s32[30]{0:T(128)S(1)}, s32[30]{0:T(128)S(1)}, u32[]{:S(2)}, u32[]{:S(2)}) collective-permute-start(s32[30]{0:T(128)S(1)} %slice.297), channel_id=1, source_target_pairs={{0,16},{16,32},{32,48},{48,64},{64,80},{80,96},{96,112},{112,128},... | collective-permute-start | bytes 368 | tf_op jit(solution)/shard_map/ppermute | solution.py:12
  11.5 4.8 %collective-permute-start.1 = (bf16[30,128]{1,0:T(8,128)(2,1)S(1)}, bf16[30,128]{1,0:T(8,128)(2,1)S(1)}, u32[]{:S(2)}, u32[]{:S(2)}) collective-permute-start(bf16[30,128]{1,0:T(8,128)(2,1)S(1)} %slice.402), channel_id=1, source_target_pairs={{0,16},{16,32},{32,48},{48,64},{64,80},{80,96},{96,112},{112,128},... | collective-permute-start | bytes 23048 | tf_op jit(solution)/shard_map/ppermute | solution.py:12
  16.3 25.3 %copy-start.6 = (s32[192,2]{0,1:T(2,128)S(1)}, s32[192,2]{0,1:T(2,128)}, u32[]{:S(2)}) copy-start(s32[192,2]{0,1:T(2,128)} %param.26) | copy-start | bytes 4612
  32.9 50.3 %copy-start.11 = (f32[2048]{0:T(1024)S(1)}, f32[2048]{0:T(1024)}, u32[]{:S(2)}) copy-start(f32[2048]{0:T(1024)} %param.20) | copy-start | bytes 24580
  32.9 50.3 %copy-start.12 = (f32[2048]{0:T(1024)S(1)}, f32[2048]{0:T(1024)}, u32[]{:S(2)}) copy-start(f32[2048]{0:T(1024)} %param.19) | copy-start | bytes 24580
  32.9 38.6 %all-to-all-start = ((bf16[16,192,128]{2,1,0:T(8,128)(2,1)}), bf16[16,192,128]{2,1,0:T(8,128)(2,1)S(1)}, u32[]{:S(2)}, u32[]{:S(2)}) async-start(bf16[16,192,128]{2,1,0:T(8,128)(2,1)} %bitcast.147), calls=%async_computation | async-start | bytes 1572864 | tf_op jit(solution)/shard_map/all_to_all | solution.py:61
  72.1 18.0 %copy-start.7 = (f32[2048]{0:T(1024)S(1)}, f32[2048]{0:T(1024)}, u32[]{:S(2)}) copy-start(f32[2048]{0:T(1024)} %param.23) | copy-start | bytes 24580
  88.9 1.1 copy-start.1
  93.3 31.3 %copy-start.10 = (bf16[1,2048,512]{2,1,0:T(8,128)(2,1)S(1)}, bf16[1,2048,512]{2,1,0:T(8,128)(2,1)}, u32[]{:S(2)}) copy-start(bf16[1,2048,512]{2,1,0:T(8,128)(2,1)} %param.27) | copy-start | bytes 6291460
  123.5 1.2 copy-start.3
  131.8 4.7 %copy-start.8 = (bf16[2048,2]{0,1:T(2,128)(2,1)S(1)}, bf16[2048,2]{0,1:T(2,128)(2,1)}, u32[]{:S(2)}) copy-start(bf16[2048,2]{0,1:T(2,128)(2,1)} %param.24) | copy-start | bytes 24580
  131.8 5.1 %copy-start.5 = (bf16[2048,16]{0,1:T(8,128)(2,1)S(1)}, bf16[2048,16]{0,1:T(8,128)(2,1)}, u32[]{:S(2)}) copy-start(bf16[2048,16]{0,1:T(8,128)(2,1)} %param.25) | copy-start | bytes 196612
  131.8 27.7 %all-to-all-start.2 = ((bf16[16,24,2048]{2,1,0:T(8,128)(2,1)}), bf16[16,24,2048]{2,1,0:T(8,128)(2,1)}, u32[]{:S(2)}, u32[]{:S(2)}) async-start(bf16[16,24,2048]{2,1,0:T(8,128)(2,1)} %bitcast.148), calls=%async_computation.2 | async-start | bytes 3145728 | tf_op jit(solution)/shard_map/all_to_all | solution.py:124
  170.9 6.2 %copy-start.2 = (f32[192,2048]{1,0:T(8,128)S(1)}, f32[192,2048]{1,0:T(8,128)}, u32[]{:S(2)}) copy-start(f32[192,2048]{1,0:T(8,128)} %copy-done.1) | copy-start | bytes 4718596
Sparse Core Ops, SparseCore 0:
  9.2 73.9 all-gather.1
where the time goes:
time: 187 us
  waiting for transfers between devices  59.9 us (32%)
  blocking collectives  30.1 us (16%)
  local copies, waits for them, and re-layouts  27.6 us (15%)
  other arithmetic  23.2 us (12%)
  starting transfers between devices  18.5 us (10%)
  between operations  13.7 us (7%)
  matrix products  13.5 us (7%)
    all_to_all x1, blocking collectives, body(): lax.all_to_all(outgoing, 'sp', split_axis=0, concat_axis=0, tiled=True)  30.1 us
    all_to_all x1, waiting for transfers between devices, body(): lax.all_to_all(convolved, 'tp', split_axis=0, concat_axis=1, tiled=True)  25 us
    all_to_all x1, waiting for transfers between devices, body(): lax.all_to_all(expert_result.reshape(senders, slot_count, features), 'sp'...  22.2 us
    convert_element_type x1, other arithmetic, body(): convolved = summed.astype(jnp.bfloat16)  16.6 us
    all_gather x1, waiting for transfers between devices, project_rows(): lax.all_gather(proj_weight, 'tp', axis=0, tiled=True)  11.1 us
    all_to_all x1, starting transfers between devices, body(): lax.all_to_all(convolved, 'tp', split_axis=0, concat_axis=1, tiled=True)  8.7 us
    gather x1, local copies, waits for them, and re-layouts, body(): returned.reshape(2 * row_count, normed.shape[1])[destination]  6.68 us
    slice x1, local copies, waits for them, and re-layouts, body(): picked[:, 0]  6.18 us
  transfers between devices with their start and end apart: 5, of which 4 were waited for; matrix products, arithmetic and copies ran while one was open for 14% of the time, Pallas kernels for 0%

commit v1 on v0

v1 whole, which is shorter than its diff:
```python
import functools

import jax
import jax.numpy as jnp
from jax import lax
from jax.experimental import pallas as pl
from jax.experimental.pallas import tpu as pltpu
from jax.sharding import PartitionSpec as P

epsilon = 1e-06
TILE = 256
CHUNK = 64
VMEM = pl.BlockSpec(memory_space=pltpu.VMEM)
SMEM = pl.BlockSpec(memory_space=pltpu.SMEM)


def params(mib):
    return pltpu.CompilerParams(vmem_limit_bytes=mib * 1024 * 1024)


def conv_kernel_body(
    starts_ref, edge_ref, value_ref, gate_ref, rim_ref, kernel_ref, out_ref, taps, rows, masked, total
):
    step = pl.program_id(0)
    tile, lanes = value_ref.shape
    tap_count = kernel_ref.shape[0]

    @pl.when(step == 0)
    def _():
        kernel = kernel_ref[...].astype(jnp.float32)
        for tap in range(tap_count):
            taps[8 * tap : 8 * tap + 8, :] = jnp.broadcast_to(kernel[tap : tap + 1, :], (8, lanes))
        rows[0:32, :] = rim_ref[...].astype(jnp.float32)

    @pl.when(step > 0)
    def _():
        rows[0:32, :] = rows[tile : tile + 32, :]

    rows[32:, :] = (
        (value_ref[...].astype(jnp.float32) * jax.nn.sigmoid(gate_ref[...].astype(jnp.float32)))
        .astype(jnp.bfloat16)
        .astype(jnp.float32)
    )

    def convolve(source, at):
        acc = jnp.zeros((CHUNK // 8, 8, lanes), jnp.float32)
        for tap in range(tap_count):
            window = source[at + 2 + tap : at + 2 + tap + CHUNK, :].reshape(CHUNK // 8, 8, lanes)
            acc = acc + window * taps[8 * tap : 8 * tap + 8, :][None]
        return acc.reshape(CHUNK, lanes)

    low, high = edge_ref[0, step], edge_ref[1, step]
    whole = jnp.logical_and(low == high, starts_ref[low] <= step * tile)

    @pl.when(whole)
    def _():
        for at in range(0, tile, CHUNK):
            out_ref[at : at + CHUNK, :] = convolve(rows, at).astype(out_ref.dtype)

    @pl.when(jnp.logical_not(whole))
    def _():
        total[...] = jnp.zeros_like(total)

        def one_document(doc, carry):
            first = starts_ref[doc] - step * tile + 2
            last = starts_ref[doc + 1] - step * tile + 2
            position = lax.broadcasted_iota(jnp.int32, rows.shape, 0)
            masked[...] = jnp.where(
                jnp.logical_and(position >= first, position < last), rows[...], jnp.float32(0.0)
            )
            for at in range(0, tile, CHUNK):
                place = lax.broadcasted_iota(jnp.int32, (CHUNK, lanes), 0) + (at + 32)
                inside = jnp.logical_and(place >= first, place < last)
                total[at : at + CHUNK, :] += jnp.where(
                    inside, convolve(masked, at), jnp.float32(0.0)
                )
            return carry

        lax.fori_loop(low, high + 1, one_document, 0)
        out_ref[...] = total[...].astype(out_ref.dtype)


def convolve_tokens(starts, edges, value, gate, rim, kernel):
    tokens, lanes = value.shape
    taps = kernel.shape[0]
    return pl.pallas_call(
        conv_kernel_body,
        grid=(tokens // TILE,),
        in_specs=[
            SMEM,
            SMEM,
            pl.BlockSpec((TILE, lanes), lambda i: (i, 0)),
            pl.BlockSpec((TILE, lanes), lambda i: (i, 0)),
            pl.BlockSpec((32, lanes), lambda i: (0, 0)),
            pl.BlockSpec((taps, lanes), lambda i: (0, 0)),
        ],
        out_specs=pl.BlockSpec((TILE, lanes), lambda i: (i, 0)),
        out_shape=jax.ShapeDtypeStruct((tokens, lanes), jnp.bfloat16),
        scratch_shapes=[
            pltpu.VMEM((8 * taps, lanes), jnp.float32),
            pltpu.VMEM((TILE + 32, lanes), jnp.float32),
            pltpu.VMEM((TILE + 32, lanes), jnp.float32),
            pltpu.VMEM((TILE, lanes), jnp.float32),
        ],
        compiler_params=params(8),
        name="gated_conv",
    )(starts, edges, value, gate, rim, kernel)


def slots_body(capacity, routing_ref, routing_t_ref, spread_ref, first_ref, second_ref):
    count = routing_ref.shape[0]
    slots = spread_ref.shape[0]
    row = lax.broadcasted_iota(jnp.int32, (count, count), 0)
    column = lax.broadcasted_iota(jnp.int32, (count, count), 1)

    def ones(mask):
        return jnp.where(mask, jnp.float32(1.0), jnp.float32(0.0))

    lane = lax.broadcasted_iota(jnp.int32, (count, 128), 1)
    one, two = routing_ref[:, 0:1], routing_ref[:, 1:2]
    named = jnp.logical_or(lane == one, lane == two)
    before = jnp.dot(
        ones(column < row).astype(jnp.bfloat16),
        ones(named).astype(jnp.bfloat16),
        preferred_element_type=jnp.float32,
    )
    slot = lax.broadcasted_iota(jnp.int32, (count, slots), 1)
    for chosen, out in ((one, first_ref), (two, second_ref)):
        place = jnp.sum(jnp.where(lane == chosen, before, 0.0), axis=1, keepdims=True)
        target = chosen * capacity + place.astype(jnp.int32)
        out[...] = ones(slot == target).astype(jnp.bfloat16)

    sub = lax.broadcasted_iota(jnp.int32, (16, count), 0)
    one, two = routing_t_ref[0:1, :], routing_t_ref[1:2, :]
    named = jnp.logical_or(sub == one, sub == two)
    before = jnp.dot(
        ones(named).astype(jnp.bfloat16),
        ones(row < column).astype(jnp.bfloat16),
        preferred_element_type=jnp.float32,
    )
    slot = lax.broadcasted_iota(jnp.int32, (slots, count), 0)
    targets = []
    for chosen in (one, two):
        place = jnp.sum(jnp.where(sub == chosen, before, 0.0), axis=0, keepdims=True)
        targets.append(chosen * capacity + place.astype(jnp.int32))
    spread_ref[...] = ones(jnp.logical_or(slot == targets[0], slot == targets[1])).astype(
        jnp.bfloat16
    )


def project_body(
    groups,
    experts,
    raw_ref,
    weight_ref,
    gain_ref,
    bias_ref,
    residual_ref,
    gain_moe_ref,
    router_ref,
    routing_ref,
    spread_ref,
    state_ref,
    outgoing_ref,
    mix_ref,
    active,
    weight,
    sem,
):
    parts, count, lanes = raw_ref.shape
    width = parts * lanes
    pieces = weight.shape[0] // 512
    copies = []
    for piece in range(pieces):
        copy = pltpu.make_async_copy(
            weight_ref.at[512 * piece : 512 * piece + 512, :],
            weight.at[512 * piece : 512 * piece + 512, :],
            sem.at[piece],
        )
        copy.start()
        copies.append(copy)
    summed = jnp.zeros((count, lanes), jnp.float32)
    for part in range(parts):
        summed = summed + raw_ref[part].astype(jnp.float32)
    average = jnp.sum(summed, axis=1, keepdims=True) * jnp.float32(1.0 / width)
    squares = jnp.zeros((count, lanes), jnp.float32)
    for part in range(parts):
        centered = raw_ref[part].astype(jnp.float32) - average
        squares = squares + centered * centered
    variance = jnp.sum(squares, axis=1, keepdims=True) * jnp.float32(1.0 / width)
    scale = lax.rsqrt(variance + epsilon)
    for part in range(parts):
        at = slice(part * lanes, part * lanes + lanes)
        value = (raw_ref[part].astype(jnp.float32) - average) * scale * gain_ref[:, at] + bias_ref[
            :, at
        ]
        active[:, at] = jax.nn.silu(value).astype(jnp.bfloat16)
    projected = residual_ref[...].astype(jnp.float32)
    for piece in range(pieces):
        copies[piece].wait()
        at = slice(512 * piece, 512 * piece + 512)
        projected = projected + jnp.dot(
            active[:, at], weight[at, :], preferred_element_type=jnp.float32
        )
    state = projected.astype(jnp.bfloat16)
    state_ref[...] = state
    state = state.astype(jnp.float32)
    power = jnp.mean(state * state, axis=1, keepdims=True)
    normed = (state * lax.rsqrt(power + epsilon) * gain_moe_ref[...]).astype(jnp.bfloat16)
    outgoing_ref[...] = jnp.dot(
        spread_ref[...], normed, preferred_element_type=jnp.float32
    ).astype(jnp.bfloat16)
    logits = jnp.dot(normed, router_ref[...], preferred_element_type=jnp.float32)
    lane = lax.broadcasted_iota(jnp.int32, logits.shape, 1)
    one, two = routing_ref[:, 0:1], routing_ref[:, 1:2]
    group = one // (experts // groups)

    def pick(mask, array):
        return jnp.sum(jnp.where(mask, array, jnp.float32(0.0)), axis=1, keepdims=True)

    raised = jnp.exp(logits)
    in_groups = jnp.logical_and(lane >= experts, lane < experts + groups)
    group_prob = pick(lane == experts + group, raised) / pick(in_groups, raised)
    first = jnp.exp(pick(lane == one, logits))
    second = jnp.exp(pick(lane == two, logits))
    both = first + second
    mix_ref[...] = jnp.where(
        lane == 0, group_prob * first / both, jnp.where(lane == 1, group_prob * second / both, 0.0)
    )


def experts_body(rows_ref, gate_ref, up_ref, down_ref, out_ref):
    rows = rows_ref[...]
    gate = jnp.dot(rows, gate_ref[...], preferred_element_type=jnp.float32)
    up = jnp.dot(rows, up_ref[...], preferred_element_type=jnp.float32)
    hidden = (jax.nn.silu(gate) * up).astype(jnp.bfloat16)
    out_ref[...] = jnp.dot(hidden, down_ref[...], preferred_element_type=jnp.float32).astype(
        jnp.bfloat16
    )


def mix_body(state_ref, returned_ref, first_ref, second_ref, mix_ref, out_ref):
    returned = returned_ref[...]
    first = jnp.dot(first_ref[...], returned, preferred_element_type=jnp.float32)
    second = jnp.dot(second_ref[...], returned, preferred_element_type=jnp.float32)
    mixture = mix_ref[:, 0:1] * first + mix_ref[:, 1:2] * second
    out_ref[...] = (state_ref[...].astype(jnp.float32) + mixture).astype(jnp.bfloat16)


def shifted(array, axis, by):
    count = lax.axis_size(axis)
    pairs = [(i, i + by) for i in range(count) if 0 <= i + by < count]
    return lax.ppermute(array, axis, pairs)


def body(
    conv_value,
    conv_gate,
    doc_ids,
    conv_kernel,
    norm_gain_conv,
    norm_bias_conv,
    proj_weight,
    residual,
    norm_gain_moe,
    group_router,
    expert_router,
    routing,
    expert_gate_w,
    expert_up_w,
    expert_down_w,
):
    tokens, lanes = conv_value.shape
    rim = conv_kernel.shape[0] - 1
    count, width = residual.shape
    groups, experts = group_router.shape[1], expert_router.shape[1]
    slots = 2 * count
    capacity = slots // experts

    tail = slice(tokens - 32, tokens)
    tail_values = (
        conv_value[tail].astype(jnp.float32) * jax.nn.sigmoid(conv_gate[tail].astype(jnp.float32))
    ).astype(jnp.bfloat16)
    tail_ids = jnp.broadcast_to(doc_ids[tail][:, None], (32, lanes)).astype(jnp.bfloat16)
    came = shifted(jnp.concatenate([tail_values, tail_ids], axis=0), "sp", 1)
    rim_values, rim_ids = came[:32], came[64 - rim :, 0].astype(jnp.int32)
    padded_ids = jnp.concatenate([rim_ids, doc_ids], axis=0)
    bounds = jnp.arange(24, dtype=jnp.int32)
    starts = jnp.sum((padded_ids[None, :] < bounds[:, None]).astype(jnp.int32), axis=1)
    tiles = doc_ids.reshape(tokens // TILE, TILE)
    edges = jnp.stack([tiles[:, 0], tiles[:, -1]])
    convolved = convolve_tokens(starts, edges, conv_value, conv_gate, rim_values, conv_kernel)
    raw_rows = lax.all_to_all(
        convolved.reshape(-1, count, lanes), "tp", split_axis=0, concat_axis=0, tiled=True
    )

    spread, first_pick, second_pick = pl.pallas_call(
        functools.partial(slots_body, capacity),
        in_specs=[VMEM] * 2,
        out_specs=[VMEM] * 3,
        out_shape=[
            jax.ShapeDtypeStruct((slots, count), jnp.bfloat16),
            jax.ShapeDtypeStruct((count, slots), jnp.bfloat16),
            jax.ShapeDtypeStruct((count, slots), jnp.bfloat16),
        ],
        compiler_params=params(8),
        name="slots",
    )(routing, routing.T)
    routers = jnp.concatenate(
        [
            expert_router,
            group_router,
            jnp.zeros((width, 128 - experts - groups), jnp.bfloat16),
        ],
        axis=1,
    )
    full_weight = lax.all_gather(proj_weight, "tp", axis=0, tiled=True)
    state, outgoing, mix = pl.pallas_call(
        functools.partial(project_body, groups, experts),
        in_specs=[VMEM, pl.BlockSpec(memory_space=pltpu.HBM)] + [VMEM] * 7,
        out_specs=[VMEM] * 3,
        out_shape=[
            jax.ShapeDtypeStruct((count, width), jnp.bfloat16),
            jax.ShapeDtypeStruct((slots, width), jnp.bfloat16),
            jax.ShapeDtypeStruct((count, 128), jnp.float32),
        ],
        scratch_shapes=[
            pltpu.VMEM((count, full_weight.shape[0]), jnp.bfloat16),
            pltpu.VMEM(full_weight.shape, jnp.bfloat16),
            pltpu.SemaphoreType.DMA((full_weight.shape[0] // 512,)),
        ],
        compiler_params=params(28),
        name="project",
    )(
        raw_rows,
        full_weight,
        norm_gain_conv[None, :],
        norm_bias_conv[None, :],
        residual,
        norm_gain_moe[None, :],
        routers,
        routing,
        spread,
    )
    arrived = lax.all_to_all(
        outgoing.reshape(experts, capacity, width), "sp", split_axis=0, concat_axis=0, tiled=True
    )
    result = pl.pallas_call(
        experts_body,
        in_specs=[VMEM] * 4,
        out_specs=VMEM,
        out_shape=jax.ShapeDtypeStruct((slots, width), jnp.bfloat16),
        compiler_params=params(24),
        name="experts",
    )(arrived.reshape(slots, width), expert_gate_w[0], expert_up_w[0], expert_down_w[0])
    returned = lax.all_to_all(
        result.reshape(experts, capacity, width), "sp", split_axis=0, concat_axis=0, tiled=True
    )
    return pl.pallas_call(
        mix_body,
        in_specs=[VMEM] * 5,
        out_specs=VMEM,
        out_shape=jax.ShapeDtypeStruct((count, width), jnp.bfloat16),
        compiler_params=params(16),
        name="mix",
    )(state, returned.reshape(slots, width), first_pick, second_pick, mix)


def solution(mesh):
    placed = (
        P("sp", "tp"),
        P("sp", "tp"),
        P("sp"),
        P(None, "tp"),
        P(),
        P(),
        P("tp", None),
        P(("sp", "tp"), None),
        P(),
        P(),
        P(),
        P(("sp", "tp"), None),
        P("sp", None, None),
        P("sp", None, None),
        P("sp", None, None),
    )
    return jax.shard_map(
        body, mesh=mesh, in_specs=placed, out_specs=P(("sp", "tp"), None), check_vma=False
    )
```

time: 187 us -> 159 us (0.85)
  blocking collectives: 30.1 us -> 55.1 us
  other arithmetic: 23.2 us -> 4 us
  local copies, waits for them, and re-layouts: 27.6 us -> 8.89 us
  Pallas kernels: 0 us -> 16.4 us
  matrix products: 13.5 us -> 0 us
  waiting for transfers between devices: 59.9 us -> 49.3 us
  starting transfers between devices: 18.5 us -> 10.5 us
    all_to_all x1 -> x2, blocking collectives: 30.1 us -> 55.1 us  [the longest x1 29.9 us: body(): lax.all_to_all(outgoing.reshape(experts, capacity, width), 'sp', split_ax...]
    all_to_all x2 -> x1, waiting for transfers between devices: 47.2 us -> 26.4 us  [body(): lax.all_to_all(convolved.reshape(-1, count, lanes), 'tp', split_axis=0, c...]
    convert_element_type x6 -> x2, other arithmetic: 21.1 us -> 0.85 us  [the longest x1 0.73 us: body(): tail_values = (conv_value[tail].astype(jnp.float32) * jax.nn.sigmoid(conv...]
    pallas_call x0 -> x5, Pallas kernels: none -> 16.4 us  [the longest x1 6.64 us: convolve_tokens(): pl.pallas_call(conv_kernel_body, grid=(tokens // TILE,), in_specs=[SMEM,...]
    dot_general x5 -> x0, matrix products: 13.5 us -> none  [the longest x1 5.7 us: project_rows(): jnp.dot(activated_rows, lax.all_gather(proj_weight, 'tp', axis=0, tiled=T...]
    all_gather x1, waiting for transfers between devices: 11.1 us -> 21.6 us  [body(): full_weight = lax.all_gather(proj_weight, 'tp', axis=0, tiled=True)]
    gather x2 -> x0, local copies, waits for them, and re-layouts: 9.81 us -> none  [the longest x1 6.68 us: body(): returned.reshape(2 * row_count, normed.shape[1])[destination]]
    slice x4 -> x2, local copies, waits for them, and re-layouts: 7.16 us -> 0.19 us  [the longest x1 0.19 us: body(): edges = jnp.stack([tiles[:, 0], tiles[:, -1]])]
  transfers between devices with their start and end apart: 5 -> 3, of which waited for: 4 -> 3; matrix products, arithmetic and copies ran while one was open for 14% -> 4% of each run, Pallas kernels for 0% -> 5%
where the time goes in v1:
time: 159 us; the launch traced here: 158 us
  blocking collectives  55.1 us (35%)
  waiting for transfers between devices  49.3 us (31%)
  Pallas kernels  16.4 us (10%)
  between operations  13.5 us (8%)
  starting transfers between devices  10.5 us (7%)
  local copies, waits for them, and re-layouts  8.89 us (6%)
  other arithmetic  4 us (3%)
    all_to_all x1, blocking collectives, body(): lax.all_to_all(outgoing.reshape(experts, capacity, width), 'sp', split_ax...  29.9 us
    all_to_all x1, waiting for transfers between devices, body(): lax.all_to_all(convolved.reshape(-1, count, lanes), 'tp', split_axis=0, c...  26.4 us
    all_to_all x1, blocking collectives, body(): lax.all_to_all(result.reshape(experts, capacity, width), 'sp', split_axis...  25.2 us
    all_gather x1, waiting for transfers between devices, body(): full_weight = lax.all_gather(proj_weight, 'tp', axis=0, tiled=True)  21.6 us
    all_to_all x1, starting transfers between devices, body(): lax.all_to_all(convolved.reshape(-1, count, lanes), 'tp', split_axis=0, c...  8.71 us
    unnamed x31, local copies, waits for them, and re-layouts  7.84 us
    pallas_call x1, Pallas kernels, convolve_tokens(): pl.pallas_call(conv_kernel_body, grid=(tokens // TILE,), in_specs=[SMEM,...  6.64 us
    pallas_call x1, Pallas kernels, body(): pl.pallas_call(functools.partial(project_body, groups, experts), in_specs...  4.61 us
  transfers between devices with their start and end apart: 3, of which 3 were waited for; matrix products, arithmetic and copies ran while one was open for 4% of the time, Pallas kernels for 5%

profile of v1, /device:TPU:0, one launch (start us, length us, event | category | flops | bytes accessed | tf_op | source)
XLA Modules:
  0.0 157.8 jit_solution(10458460545332503610)
XLA Ops:
  6.5 0.0 all-gather.2.cloned.1.call-start
  6.5 0.7 all-gather.2.cloned.1.call-update
  7.3 0.0 copy-start.11
  7.3 0.8 slice_convert_fusion
  8.0 0.1 pad.8.clone
  8.1 0.7 multiply_convert_fusion
  8.8 0.1 pad_maximum_fusion
  8.9 0.0 copy-start.13
  8.9 1.8 %collective-permute-start = (bf16[64,128]{1,0:T(8,128)(2,1)S(1)}, bf16[64,128]{1,0:T(8,128)(2,1)S(1)}, u32[]{:S(2)}, u32[]{:S(2)}) collective-permute-start(bf16[64,128]{1,0:T(8,128)(2,1)S(1)} %pad_maximum_fusion), channel_id=1, source_target_pairs={{0,16},{16,32},{32,48},{48,64},{64,80},{80,96},{96,112},{112,128},... | collective-permute-start | bytes 49160 | tf_op jit(solution)/shard_map/ppermute | solution.py:253
  10.7 0.7 reshape.22
  11.5 0.2 slice_reduce_fusion.1
  11.7 0.5 collective-permute-done
  12.2 0.1 convert_reduce_fusion.1
  12.3 0.8 pad_add_fusion
  13.1 0.1 convert_reduce_fusion.starts_ref
  13.2 0.0 copy-start.4
  13.2 1.1 copy-done.4
  14.4 0.0 copy-start.5
  14.4 1.1 copy-done.5
  15.5 0.7 copy-done.7
  16.2 6.6 %gated_conv.1 = bf16[3072,128]{1,0:T(8,128)(2,1)} custom-call(s32[24]{0:T(128)S(1)} %convert_reduce_fusion.starts_ref, s32[2,12]{1,0:T(2,128)S(1)} %pad_add_fusion.1.edge_ref, bf16[3072,128]{1,0:T(8,128)(2,1)S(1)} %copy-done.5, bf16[3072,128]{1,0:T(8,128)(2,1)S(1)} %copy-done.4, bf16[32,128]{1,0:T(8,128)(2,1)S(1)} %slice.33.rim_ref, ...), custom_call_target="tpu_custom_call" | custom-call | tf_op jit(solution)/shard_map/gated_conv/pallas_call | solution.py:86
  22.9 8.7 %all-to-all-start = ((bf16[16,192,128]{2,1,0:T(8,128)(2,1)}), bf16[16,192,128]{2,1,0:T(8,128)(2,1)S(1)}, u32[]{:S(2)}, u32[]{:S(2)}) async-start(bf16[16,192,128]{2,1,0:T(8,128)(2,1)} %bitcast), calls=%async_computation | async-start | bytes 1572864 | tf_op jit(solution)/shard_map/all_to_all | solution.py:293
  31.6 0.1 pad.2.clone
  31.7 0.0 copy-done.11
  31.7 0.1 copy.31.routing_ref
  31.8 0.0 copy-done.13
  31.8 0.3 copy.29
  32.1 0.0 copy-done.12
  32.1 1.0 copy.28
  33.2 0.6 slots.1
  33.7 1.4 maximum_maximum_fusion.router_ref
  35.1 26.4 %all-to-all-done.raw_ref = bf16[16,192,128]{2,1,0:T(8,128)(2,1)S(1)} async-done(((bf16[16,192,128]{2,1,0:T(8,128)(2,1)}), bf16[16,192,128]{2,1,0:T(8,128)(2,1)S(1)}, u32[]{:S(2)}, u32[]{:S(2)}) %all-to-all-start) | async-done | bytes 786464 | tf_op jit(solution)/shard_map/all_to_all | solution.py:293
  61.5 21.6 %all-gather.2.cloned.1.call-done.weight_ref = bf16[2048,2048]{1,0:T(8,128)(2,1)} async-done(((bf16[128,2048]{1,0:T(8,128)(2,1)}), bf16[2048,2048]{1,0:T(8,128)(2,1)}) %all-gather.2.cloned.1.call-update) | async-done | bytes 8388624 | tf_op jit(solution)/shard_map/all_gather | solution.py:317
  83.2 0.0 copy-done.6
  83.2 0.0 copy-done.8
  83.2 0.0 copy-done.9
  83.2 0.0 copy-done.10
  83.2 0.0 copy-start
  83.2 3.4 %copy-done = bf16[2048,2048]{1,0:T(8,128)(2,1)S(1)} copy-done((bf16[2048,2048]{1,0:T(8,128)(2,1)S(1)}, bf16[2048,2048]{1,0:T(8,128)(2,1)}, u32[]{:S(2)}) %copy-start) | copy-done | bytes 8388632
  86.6 4.6 %project.1 = (bf16[192,2048]{1,0:T(8,128)(2,1)S(1)}, bf16[384,2048]{1,0:T(8,128)(2,1)S(1)}, f32[192,128]{1,0:T(8,128)S(1)}) custom-call(bf16[16,192,128]{2,1,0:T(8,128)(2,1)S(1)} %all-to-all-done.raw_ref, bf16[2048,2048]{1,0:T(8,128)(2,1)S(1)} %copy-done, f32[1,2048]{1,0:T(1,128)S(1)} %bitcast.21, f32[1,2048]{1,0:T(1,128)S(1)} %bitcast.22, ...), custom_call_target="tpu_custom_call" | custom-call | tf_op jit(solution)/shard_map/project/pallas_call | solution.py:318
  91.2 0.0 copy-start.1
  91.2 29.9 %all_to_all.15 = bf16[16,24,2048]{2,1,0:T(8,128)(2,1)S(1)} all-to-all(bf16[16,24,2048]{2,1,0:T(8,128)(2,1)S(1)} %bitcast.20), channel_id=1, replica_groups=mesh['sp'=16,'tp'=16] {'sp'}, dimensions={0} | all-to-all | bytes 3145728 | tf_op jit(solution)/shard_map/all_to_all | solution.py:345
  121.1 0.0 copy-done.2
  121.1 0.0 copy-done.3
  121.1 0.0 copy-done.1
  121.1 2.6 %experts.1 = bf16[384,2048]{1,0:T(8,128)(2,1)S(1)} custom-call(bf16[384,2048]{1,0:T(8,128)(2,1)S(1)} %bitcast.15, bf16[2048,512]{1,0:T(8,128)(2,1)S(1)} %bitcast.17, bf16[2048,512]{1,0:T(8,128)(2,1)S(1)} %bitcast.18, bf16[512,2048]{1,0:T(8,128)(2,1)S(1)} %bitcast.19), custom_call_target="tpu_custom_call" | custom-call | tf_op jit(solution)/shard_map/experts/pallas_call | solution.py:348
  123.8 25.2 %all_to_all.16 = bf16[16,24,2048]{2,1,0:T(8,128)(2,1)S(1)} all-to-all(bf16[16,24,2048]{2,1,0:T(8,128)(2,1)S(1)} %bitcast.16), channel_id=1, replica_groups=mesh['sp'=16,'tp'=16] {'sp'}, dimensions={0} | all-to-all | bytes 3145728 | tf_op jit(solution)/shard_map/all_to_all | solution.py:356
  149.0 2.0 %mix.1 = bf16[192,2048]{1,0:T(8,128)(2,1)} custom-call(bf16[192,2048]{1,0:T(8,128)(2,1)S(1)} %get-tuple-element.12.state_ref, bf16[384,2048]{1,0:T(8,128)(2,1)S(1)} %bitcast.14, bf16[192,384]{1,0:T(8,128)(2,1)S(1)} %get-tuple-element.14.first_ref, bf16[192,384]{1,0:T(8,128)(2,1)S(1)} %get-tuple-element.15.second_ref, f32[192,128]{1,0:T(8,128)S(1)} %get-tuple-element.16.mix_ref), custom_call_target="tpu_custom_call" | custom-call | tf_op jit(solution)/shard_map/mix/pallas_call | solution.py:359
  (11 shorter events, 0.0 us)
Async XLA Ops:
  6.5 76.6 %all-gather.2.cloned.1.call-start = ((), (), s32[]{:S(2)}) async-start(), calls=%async_computation.3 | async-start | bytes 8912896 | tf_op jit(solution)/shard_map/all_gather | solution.py:317
  7.3 24.4 %copy-start.11 = (s32[192,2]{0,1:T(2,128)S(1)}, s32[192,2]{0,1:T(2,128)}, u32[]{:S(2)}) copy-start(s32[192,2]{0,1:T(2,128)} %param.26) | copy-start | bytes 4612
  8.9 22.9 %copy-start.13 = (bf16[2048,2]{0,1:T(2,128)(2,1)S(1)}, bf16[2048,2]{0,1:T(2,128)(2,1)}, u32[]{:S(2)}) copy-start(bf16[2048,2]{0,1:T(2,128)(2,1)} %param.24) | copy-start | bytes 24580
  8.9 3.3 %collective-permute-start = (bf16[64,128]{1,0:T(8,128)(2,1)S(1)}, bf16[64,128]{1,0:T(8,128)(2,1)S(1)}, u32[]{:S(2)}, u32[]{:S(2)}) collective-permute-start(bf16[64,128]{1,0:T(8,128)(2,1)S(1)} %pad_maximum_fusion), channel_id=1, source_target_pairs={{0,16},{16,32},{32,48},{48,64},{64,80},{80,96},{96,112},{112,128},... | collective-permute-start | bytes 49160 | tf_op jit(solution)/shard_map/ppermute | solution.py:253
  13.2 1.1 copy-start.4
  14.4 1.1 copy-start.5
  15.5 0.7 copy-start.7
  16.2 15.9 %copy-start.12 = (bf16[2048,16]{0,1:T(8,128)(2,1)S(1)}, bf16[2048,16]{0,1:T(8,128)(2,1)}, u32[]{:S(2)}) copy-start(bf16[2048,16]{0,1:T(8,128)(2,1)} %param.25) | copy-start | bytes 196612
  22.8 60.3 %copy-start.6 = (bf16[192,2048]{1,0:T(8,128)(2,1)S(1)}, bf16[192,2048]{1,0:T(8,128)(2,1)}, u32[]{:S(2)}) copy-start(bf16[192,2048]{1,0:T(8,128)(2,1)} %residual_ref.1) | copy-start | bytes 2359300
  22.8 60.3 %copy-start.8 = (f32[2048]{0:T(1024)S(1)}, f32[2048]{0:T(1024)}, u32[]{:S(2)}) copy-start(f32[2048]{0:T(1024)} %param.19) | copy-start | bytes 24580
  22.8 60.3 %copy-start.9 = (f32[2048]{0:T(1024)S(1)}, f32[2048]{0:T(1024)}, u32[]{:S(2)}) copy-start(f32[2048]{0:T(1024)} %param.20) | copy-start | bytes 24580
  22.8 60.3 %copy-start.10 = (f32[2048]{0:T(1024)S(1)}, f32[2048]{0:T(1024)}, u32[]{:S(2)}) copy-start(f32[2048]{0:T(1024)} %param.23) | copy-start | bytes 24580
  22.9 38.7 %all-to-all-start = ((bf16[16,192,128]{2,1,0:T(8,128)(2,1)}), bf16[16,192,128]{2,1,0:T(8,128)(2,1)S(1)}, u32[]{:S(2)}, u32[]{:S(2)}) async-start(bf16[16,192,128]{2,1,0:T(8,128)(2,1)} %bitcast), calls=%async_computation | async-start | bytes 1572864 | tf_op jit(solution)/shard_map/all_to_all | solution.py:293
  83.2 3.4 %copy-start = (bf16[2048,2048]{1,0:T(8,128)(2,1)S(1)}, bf16[2048,2048]{1,0:T(8,128)(2,1)}, u32[]{:S(2)}) copy-start(bf16[2048,2048]{1,0:T(8,128)(2,1)} %all-gather.2.cloned.1.call-done.weight_ref) | copy-start | bytes 25165828
  86.5 34.6 %copy-start.2 = (bf16[1,2048,512]{2,1,0:T(8,128)(2,1)S(1)}, bf16[1,2048,512]{2,1,0:T(8,128)(2,1)}, u32[]{:S(2)}) copy-start(bf16[1,2048,512]{2,1,0:T(8,128)(2,1)} %param.28) | copy-start | bytes 6291460
  86.5 34.6 %copy-start.3 = (bf16[1,512,2048]{2,1,0:T(8,128)(2,1)S(1)}, bf16[1,512,2048]{2,1,0:T(8,128)(2,1)}, u32[]{:S(2)}) copy-start(bf16[1,512,2048]{2,1,0:T(8,128)(2,1)} %param.29) | copy-start | bytes 6291460
  91.2 29.9 %copy-start.1 = (bf16[1,2048,512]{2,1,0:T(8,128)(2,1)S(1)}, bf16[1,2048,512]{2,1,0:T(8,128)(2,1)}, u32[]{:S(2)}) copy-start(bf16[1,2048,512]{2,1,0:T(8,128)(2,1)} %param.27) | copy-start | bytes 6291460
Sparse Core Ops, SparseCore 0:
  9.2 73.9 all-gather.1
